TPU v7x, 32 devices: a whole 2x2x4 slice. The times are simulated.
32 devices in a mesh: ep: 8 (over z, x), tp: 4 (over y, core).
Axes of the slice: x: 2, y: 2, z: 4, core: 2. Of those that a mesh axis runs over, the one named last changes fastest.
Arguments:
- tokens: bfloat16 [8192, 2048], P(('ep', 'tp')), may hold values from -6 to 6
- pre_gain: float32 [2048], replicated, may hold values from 0.1 to 1.9
- post_gain: float32 [2048], replicated, may hold values from 0.1 to 1.9
- expert_ids: int32 [8192, 2], P(('ep', 'tp')), may hold values from 0 to 7, as said below
- route_weight: float32 [8192, 2], P(('ep', 'tp')), may hold values from 0.1 to 1
- w_gate: bfloat16 [8, 2048, 512], P('ep', None, 'tp'), may hold values from -0.125 to 0.125
- w_up: bfloat16 [8, 2048, 512], P('ep', None, 'tp'), may hold values from -0.125 to 0.125
- w_down: bfloat16 [8, 2048, 512], P('ep', None, 'tp'), may hold values from -0.25 to 0.25
Outputs:
- layer_out: bfloat16 [8192, 2048], P(('ep', 'tp'))
Inputs may be any that keep to these rules, and one draw needn't show every extreme that they name: `expert_ids`: each token names two different experts of one group, group g being experts 4 * g to 4 * g + 3. Among the rows of one device (aligned blocks of 256 rows) no expert is named more than 128 times, and in every block some expert is named exactly 128 times; one expert is named 128 times in every block.
All inputs are finite; a program needn't handle non-finite values.
Results may differ from a plain program's by a relative error of at most 0.0071.
Values may be sent and summed in bfloat16 or wider, within the bound.
A program may use at most 64 MiB of HBM per device.

v0:
```python
import jax
import jax.numpy as jnp
from jax import lax
from jax.sharding import PartitionSpec as P


def rms_scale(values, gain):
    mean_sq = jnp.mean(values * values, axis=-1, keepdims=True)
    return values * lax.rsqrt(mean_sq + 1e-06) * gain


def expert_terms(rows, gate_part, up_part, down_part):
    gate = jnp.dot(rows, gate_part, preferred_element_type=jnp.float32)
    up = jnp.dot(rows, up_part, preferred_element_type=jnp.float32)
    hidden = (jax.nn.silu(gate) * up).astype(jnp.bfloat16)
    return lax.dot_general(
        hidden, down_part, (((1,), (1,)), ((), ())), preferred_element_type=jnp.float32
    )


def collect_expert(w_gate, w_up, w_down):
    return (
        lax.all_gather(w_gate, "tp", axis=2, tiled=True),
        lax.all_gather(w_up, "tp", axis=2, tiled=True),
        lax.all_gather(w_down, "tp", axis=2, tiled=True),
    )


def body(tokens, pre_gain, post_gain, expert_ids, route_weight, w_gate, w_up, w_down):
    count, width = tokens.shape
    top = expert_ids.shape[1]
    experts = lax.axis_size("ep") * w_gate.shape[0]
    capacity = 2 * top * count // experts
    normed = rms_scale(tokens.astype(jnp.float32), pre_gain).astype(jnp.bfloat16)
    flat = expert_ids.reshape(-1)
    onehot = (flat[:, None] == jnp.arange(experts, dtype=jnp.int32)[None, :]).astype(jnp.int32)
    rank = jnp.sum((jnp.cumsum(onehot, axis=0) - onehot) * onehot, axis=1)
    target = flat * capacity + rank
    source = jnp.full((experts * capacity,), count, jnp.int32)
    source = source.at[target].set(jnp.arange(count * top, dtype=jnp.int32) // top)
    padded = jnp.concatenate([normed, jnp.zeros((1, width), jnp.bfloat16)], axis=0)
    outgoing = padded[source].reshape(experts, capacity, width)
    arrived = lax.all_to_all(outgoing, "ep", split_axis=0, concat_axis=0, tiled=True)
    rows = arrived.reshape(experts * capacity, width)
    gate_all, up_all, down_all = collect_expert(w_gate, w_up, w_down)
    result = expert_terms(rows, gate_all[0], up_all[0], down_all[0])
    answer = result.astype(jnp.bfloat16).reshape(experts, capacity, width)
    returned = lax.all_to_all(answer, "ep", split_axis=0, concat_axis=0, tiled=True)
    per_route = returned.reshape(experts * capacity, width)[target].reshape(count, top, width)
    mixed = jnp.sum(per_route.astype(jnp.float32) * route_weight[:, :, None], axis=1)
    return rms_scale(mixed, post_gain).astype(jnp.bfloat16)


def solution(mesh):
    in_specs = (
        P(("ep", "tp"), None),
        P(),
        P(),
        P(("ep", "tp"), None),
        P(("ep", "tp"), None),
        P("ep", None, "tp"),
        P("ep", None, "tp"),
        P("ep", None, "tp"),
    )
    out_specs = P(("ep", "tp"), None)
    return jax.shard_map(body, mesh=mesh, in_specs=in_specs, out_specs=out_specs, check_vma=False)
```

profile of v0, /device:TPU:0, one launch (start us, length us, event | category | flops | bytes accessed | tf_op | source)
XLA Modules:
  0.0 263.1 jit_solution(6844710715102796030)
XLA Ops:
  6.5 0.7 all-gather.6.cloned.1.call-update
  7.3 0.8 copy.11
  8.1 0.7 broadcast_multiply_fusion
  8.9 1.5 fusion
  10.4 1.1 reduce-window.6
  11.6 0.2 slice_reduce_fusion
  12.3 0.3 fusion.2
  12.8 2.4 scatter_custom_fusion
  15.3 6.0 %gather_fusion = bf16[1024,2048]{1,0:T(8,128)(2,1)} fusion(bf16[257,2048]{1,0:T(8,128)(2,1)S(1)} %concatenate.3, s32[1024]{0:T(1024)S(1)} %fusion.15), kind=kCustom, calls=%fused_computation | custom fusion | bytes 8392704 | tf_op jit(solution)/shard_map/gather | solution.py:42
  21.3 7.3 %all-to-all-start = ((bf16[8,128,2048]{2,1,0:T(8,128)(2,1)}), bf16[8,128,2048]{2,1,0:T(8,128)(2,1)}, u32[]{:S(2)}, u32[]{:S(2)}) async-start(bf16[8,128,2048]{2,1,0:T(8,128)(2,1)} %bitcast.29), calls=%async_computation | async-start | bytes 8388608 | tf_op jit(solution)/shard_map/all_to_all | solution.py:43
  28.6 0.7 all-gather.4.cloned.1.call-update
  29.4 0.7 all-gather.8.cloned.1.call-update
  30.1 4.4 %all-gather.6.cloned.1.call-done = bf16[1,2048,512]{2,1,0:T(8,128)(2,1)} async-done(((bf16[1,2048,128]{2,1,0:T(8,128)(2,1)}), bf16[1,2048,512]{2,1,0:T(8,128)(2,1)}) %all-gather.6.cloned.1.call-update) | async-done | bytes 2097168 | tf_op jit(solution)/shard_map/all_gather | solution.py:24
  34.5 87.4 %all-to-all-done = bf16[8,128,2048]{2,1,0:T(8,128)(2,1)} async-done(((bf16[8,128,2048]{2,1,0:T(8,128)(2,1)}), bf16[8,128,2048]{2,1,0:T(8,128)(2,1)}, u32[]{:S(2)}, u32[]{:S(2)}) %all-to-all-start) | async-done | bytes 4194336 | tf_op jit(solution)/shard_map/all_to_all | solution.py:43
  121.9 5.2 %fusion.4 = f32[1024,512]{1,0:T(8,128)S(1)} fusion(bf16[1024,2048]{1,0:T(8,128)(2,1)} %bitcast.5, bf16[1,2048,512]{2,1,0:T(8,128)(2,1)} %all-gather.6.cloned.1.call-done), kind=kOutput, calls=%fused_computation.11 | convolution fusion | flops 2147483648 | bytes 8388608 | tf_op jit(solution)/shard_map/dot_general | solution.py:14
  127.1 10.1 %convolution_convert_fusion = bf16[1024,2048]{1,0:T(8,128)(2,1)} fusion(bf16[1,2048,512]{2,1,0:T(8,128)(2,1)} %all-gather.8.cloned.1.call-done, f32[1024,512]{1,0:T(8,128)S(1)} %fusion.4, bf16[1024,2048]{1,0:T(8,128)(2,1)} %bitcast.5, bf16[1,2048,512]{2,1,0:T(8,128)(2,1)} %all-gather.4.cloned.1.call-done), kind=kOutput, calls=%fused_computation.4 | convolution fusion | flops 4300210176 | bytes 14680064 | tf_op jit(solution)/shard_map/dot_general | solution.py:16
  137.3 4.9 %all-to-all-start.1 = ((bf16[8,128,2048]{2,1,0:T(8,128)(2,1)}), bf16[8,128,2048]{2,1,0:T(8,128)(2,1)}, u32[]{:S(2)}, u32[]{:S(2)}) async-start(bf16[8,128,2048]{2,1,0:T(8,128)(2,1)} %bitcast.30), calls=%async_computation.1 | async-start | bytes 8388608 | tf_op jit(solution)/shard_map/all_to_all | solution.py:48
  142.3 92.3 %all-to-all-done.1 = bf16[8,128,2048]{2,1,0:T(8,128)(2,1)} async-done(((bf16[8,128,2048]{2,1,0:T(8,128)(2,1)}), bf16[8,128,2048]{2,1,0:T(8,128)(2,1)}, u32[]{:S(2)}, u32[]{:S(2)}) %all-to-all-start.1) | async-done | bytes 4194336 | tf_op jit(solution)/shard_map/all_to_all | solution.py:48
  234.6 7.1 %gather_fusion.1 = bf16[512,2048]{1,0:T(8,128)(2,1)S(1)} fusion(bf16[1024,2048]{1,0:T(8,128)(2,1)} %bitcast.10, s32[1024]{0:T(1024)S(1)} %pad_clamp_fusion), kind=kCustom, calls=%fused_computation.1 | custom fusion | bytes 4196352 | tf_op jit(solution)/shard_map/gather | solution.py:49
  241.7 4.0 %reshape.85 = f32[256,2,2048]{2,1,0:T(2,128)} reshape(bf16[512,2048]{1,0:T(8,128)(2,1)S(1)} %gather_fusion.1) | data formatting | bytes 6291456 | tf_op jit(solution)/shard_map/convert_element_type | solution.py:50
  245.7 8.9 %multiply_reduce_fusion = f32[256,2048]{1,0:T(8,128)S(1)} fusion(f32[256,2,2048]{2,1,0:T(2,128)} %reshape.85, f32[256,2]{1,0:T(8,128)S(1)} %copy.13), kind=kLoop, calls=%fused_computation.3 | loop fusion | flops 1572864 | bytes 6293504 | tf_op jit(solution)/shard_map/reduce_sum | solution.py:50
  254.6 0.2 multiply_reduce_fusion.1
  254.9 0.5 copy-done.2
  255.3 1.2 multiply_convert_fusion
  (28 shorter events, 1.1 us)
Async XLA Ops:
  6.5 5.7 %copy-start = (bf16[256,2048]{1,0:T(8,128)(2,1)S(1)}, bf16[256,2048]{1,0:T(8,128)(2,1)}, u32[]{:S(2)}) copy-start(bf16[256,2048]{1,0:T(8,128)(2,1)} %param.8) | copy-start | bytes 3145732
  6.5 5.8 %copy-start.1 = (f32[2048]{0:T(1024)S(1)}, f32[2048]{0:T(1024)}, u32[]{:S(2)}) copy-start(f32[2048]{0:T(1024)} %param.9) | copy-start | bytes 24580
  6.5 27.9 %all-gather.6.cloned.1.call-start = ((), (), s32[]{:S(2)}) async-start(), calls=%async_computation.3 | async-start | bytes 2621440 | tf_op jit(solution)/shard_map/all_gather | solution.py:24
  21.3 100.6 %all-to-all-start = ((bf16[8,128,2048]{2,1,0:T(8,128)(2,1)}), bf16[8,128,2048]{2,1,0:T(8,128)(2,1)}, u32[]{:S(2)}, u32[]{:S(2)}) async-start(bf16[8,128,2048]{2,1,0:T(8,128)(2,1)} %bitcast.29), calls=%async_computation | async-start | bytes 8388608 | tf_op jit(solution)/shard_map/all_to_all | solution.py:43
  28.6 98.5 %all-gather.4.cloned.1.call-start = ((), (), s32[]{:S(2)}) async-start(), calls=%async_computation.2 | async-start | bytes 2621440 | tf_op jit(solution)/shard_map/all_gather | solution.py:23
  29.3 97.8 %all-gather.8.cloned.1.call-start = ((), (), s32[]{:S(2)}) async-start(), calls=%async_computation.4 | async-start | bytes 2621440 | tf_op jit(solution)/shard_map/all_gather | solution.py:25
  137.3 4.9 %copy-start.3 = (f32[256,2]{0,1:T(2,128)S(1)}, f32[256,2]{0,1:T(2,128)}, u32[]{:S(2)}) copy-start(f32[256,2]{0,1:T(2,128)} %param.12) | copy-start | bytes 6148
  137.3 97.3 %all-to-all-start.1 = ((bf16[8,128,2048]{2,1,0:T(8,128)(2,1)}), bf16[8,128,2048]{2,1,0:T(8,128)(2,1)}, u32[]{:S(2)}, u32[]{:S(2)}) async-start(bf16[8,128,2048]{2,1,0:T(8,128)(2,1)} %bitcast.30), calls=%async_computation.1 | async-start | bytes 8388608 | tf_op jit(solution)/shard_map/all_to_all | solution.py:48
  254.6 0.7 copy-start.2
Sparse Core Ops, SparseCore 0:
  8.9 25.5 all-gather.5
  36.0 22.8 all-gather.3
  60.4 22.8 all-gather.7
where the time goes:
time: 264 us; the launch traced here: 263 us
  waiting for transfers between devices  186 us (70%)
  local copies, waits for them, and re-layouts  21.9 us (8%)
  matrix products  15.3 us (6%)
  other arithmetic  14.1 us (5%)
  between operations  13.3 us (5%)
  starting transfers between devices  12.2 us (5%)
    all_to_all x1, waiting for transfers between devices, body(): lax.all_to_all(answer, 'ep', split_axis=0, concat_axis=0, tiled=True)  92.3 us
    all_to_all x1, waiting for transfers between devices, body(): lax.all_to_all(outgoing, 'ep', split_axis=0, concat_axis=0, tiled=True)  87.4 us
    dot_general x1, matrix products, expert_terms(): lax.dot_general(hidden, down_part, (((1,), (1,)), ((), ())), preferred_el...  10.1 us
    reduce_sum x1, other arithmetic, body(): jnp.sum(per_route.astype(jnp.float32) * route_weight[:, :, None], axis=1)  8.89 us
    all_to_all x1, starting transfers between devices, body(): lax.all_to_all(outgoing, 'ep', split_axis=0, concat_axis=0, tiled=True)  7.28 us
    gather x1, local copies, waits for them, and re-layouts, body(): returned.reshape(experts * capacity, width)[target]  7.13 us
    gather x1, local copies, waits for them, and re-layouts, body(): outgoing = padded[source].reshape(experts, capacity, width)  6.03 us
  transfers between devices with their start and end apart: 5, of which 3 were waited for; matrix products, arithmetic and copies ran while one was open for 7% of the time, Pallas kernels for 0%

commit v1 on v0

--- a/solution.py
+++ b/solution.py
@@ -1,6 +1,10 @@
+import functools
+
 import jax
 import jax.numpy as jnp
 from jax import lax
+from jax.experimental import pallas as pl
+from jax.experimental.pallas import tpu as pltpu
 from jax.sharding import PartitionSpec as P
 
 
@@ -50,6 +54,280 @@
     mixed = jnp.sum(per_route.astype(jnp.float32) * route_weight[:, :, None], axis=1)
     return rms_scale(mixed, post_gain).astype(jnp.bfloat16)
 
+MESH = pl.DeviceIdType.MESH
+GU_CUTS = 2
+DOWN_CUTS = 4
+VMEM_BYTES = 60 * 2**20
+
+
+def flip(index, stride):
+    return index + stride - 2 * stride * lax.rem(lax.div(index, stride), 2)
+
+
+def kernel(
+    n_ep, tok, pre, post, wr, wg, wu, wd, out,
+    T, X, WR, COL, GU, DN, H, S, R, PZ, ZS, ZR, ACC,
+    loc, t_send, t_recv, w_send, w_recv, g_send, g_recv, d_send, d_recv, x_send, x_recv, z_send, z_recv,
+):
+    count, width = tok.shape
+    part = wg.shape[2]
+    experts = wr.shape[0]
+    half = n_ep // 2
+    e, t = lax.axis_index("ep"), lax.axis_index("tp")
+    to_x, to_z, to_h = (flip(e, 1), t), (flip(e, 2), t), (flip(e, half), t)
+    to_c, to_y = (e, flip(t, 1)), (e, flip(t, 2))
+
+    barrier = pltpu.get_barrier_semaphore()
+    for who in (to_x, to_z, to_h, to_c, to_y):
+        pl.semaphore_signal(barrier, inc=1, device_id=who, device_id_type=MESH)
+
+    own = [
+        pltpu.make_async_copy(tok, T.at[0], loc.at[0]),
+        pltpu.make_async_copy(wr, WR.at[0], loc.at[1]),
+        pltpu.make_async_copy(wg.at[0], GU.at[0, :, pl.ds(0, part)], loc.at[2]),
+        pltpu.make_async_copy(wu.at[0], GU.at[0, :, pl.ds(part, part)], loc.at[3]),
+        pltpu.make_async_copy(wd.at[0], DN.at[:, pl.ds(0, part)], loc.at[4]),
+    ]
+    for copy in own:
+        copy.start()
+
+    def remote(src, dst, send, recv, who):
+        return pltpu.make_async_remote_copy(
+            src_ref=src, dst_ref=dst, send_sem=send, recv_sem=recv, device_id=who, device_id_type=MESH
+        )
+
+    block_from = {1: (0, to_z), 2: (0, to_x), 3: (1, to_x)}
+    sent = []
+
+    def tokens_copy(k):
+        s, who = block_from[k]
+        return (
+            remote(WR.at[s], WR.at[k], w_send.at[k], w_recv.at[k], who),
+            remote(T.at[s], T.at[k], t_send.at[k], t_recv.at[k], who),
+        )
+
+    def route(k):
+        if k % 2:
+            return k - 1, to_c
+        if k % 4:
+            return k - 2, to_y
+        return 0, to_h
+
+    g_rows, d_rows = width // GU_CUTS, width // DOWN_CUTS
+
+    def gu_copy(k, j):
+        s, who = route(k)
+        rows = pl.ds(j * g_rows, g_rows)
+        return (remote(GU.at[s, rows], GU.at[k, rows], g_send.at[k, j], g_recv.at[k, j], who),)
+
+    def dn_copy(k, j):
+        s, who = route(k)
+        rows = pl.ds(j * d_rows, d_rows)
+        return (
+            remote(
+                DN.at[rows, pl.ds(s * part, part)], DN.at[rows, pl.ds(k * part, part)],
+                d_send.at[k, j], d_recv.at[k, j], who,
+            ),
+        )
+
+    def go(copies):
+        for copy in copies:
+            copy.start()
+            sent.append(copy)
+
+    def arrive(copies):
+        for copy in copies:
+            copy.wait_recv()
+
+    def norm(block):
+        rows = pl.ds(block * count, count)
+
+        def some(i, carry):
+            part_rows = pl.ds(pl.multiple_of(i * 32, 32), 32)
+            values = T[block, part_rows, :].astype(jnp.float32)
+            X[block, part_rows, :] = rms_scale(values, pre[...]).astype(jnp.bfloat16)
+            return carry
+
+        lax.fori_loop(0, count // 32, some, 0)
+        eye = lax.broadcasted_iota(jnp.int32, (count, count), 0) == lax.broadcasted_iota(
+            jnp.int32, (count, count), 1
+        )
+        which = lax.broadcasted_iota(jnp.int32, (experts, count), 0)
+        table = WR[block]
+        for h in range(2):
+            expert = lax.rem(e + h * half, n_ep)
+            row = jnp.sum(jnp.where(which == expert, table, 0.0), axis=0, keepdims=True)
+            col = jnp.sum(jnp.where(eye, row, 0.0), axis=1, keepdims=True)
+            COL[h, rows, :] = jnp.broadcast_to(col, (count, part))
+
+    def hidden(slots, blocks):
+        low, high = slots
+        first, last = blocks
+        span = last - first
+
+        def one(i, carry):
+            s = low + lax.div(i, span)
+            b = first + lax.rem(i, span)
+            rows = pl.ds(pl.multiple_of(b * count, count), count)
+            both = jnp.dot(X[b], GU[s], preferred_element_type=jnp.float32)
+            gate, up = both[:, :part], both[:, part:]
+            value = gate / (1.0 + jnp.exp(-gate)) * up * COL[lax.div(s, 4), rows, :]
+            H[rows, pl.ds(pl.multiple_of(s * part, part), part)] = value.astype(jnp.bfloat16)
+            return carry
+
+        lax.fori_loop(0, (high - low) * span, one, 0)
+
+    for copy in own[:2]:
+        copy.wait()
+    pl.semaphore_wait(barrier, 5)
+    go(tokens_copy(1))
+    go(tokens_copy(2))
+    for copy in own[2:4]:
+        copy.wait()
+    for j in range(GU_CUTS):
+        for k in (4, 2, 1):
+            go(gu_copy(k, j))
+    own[4].wait()
+    for j in range(DOWN_CUTS):
+        for k in (4, 2, 1):
+            go(dn_copy(k, j))
+    norm(0)
+    for j in range(GU_CUTS):
+        arrive(gu_copy(1, j))
+    hidden((0, 2), (0, 1))
+    arrive(tokens_copy(1))
+    go(tokens_copy(3))
+    norm(1)
+    for j in range(GU_CUTS):
+        arrive(gu_copy(2, j))
+        go(gu_copy(3, j))
+    arrive(tokens_copy(2))
+    norm(2)
+    hidden((0, 2), (1, 3))
+    for j in range(GU_CUTS):
+        arrive(gu_copy(4, j))
+        go(gu_copy(6, j))
+        go(gu_copy(5, j))
+    for j in range(GU_CUTS):
+        arrive(gu_copy(3, j))
+    hidden((2, 4), (0, 3))
+    for j in range(DOWN_CUTS):
+        arrive(dn_copy(2, j))
+        go(dn_copy(3, j))
+    for j in range(GU_CUTS):
+        arrive(gu_copy(5, j))
+    hidden((4, 6), (0, 3))
+    arrive(tokens_copy(3))
+    norm(3)
+    hidden((0, 6), (3, 4))
+    for j in range(GU_CUTS):
+        arrive(gu_copy(6, j))
+        go(gu_copy(7, j))
+    arrive(dn_copy(4, 0))
+    go(dn_copy(6, 0))
+    go(dn_copy(5, 0))
+    hidden((6, 7), (0, 4))
+    for j in range(GU_CUTS):
+        arrive(gu_copy(7, j))
+    hidden((7, 8), (0, 4))
+
+    def down(block, j):
+        return lax.dot_general(
+            H[pl.ds(block * count, count), :], DN[pl.ds(j * d_rows, d_rows), :],
+            (((1,), (1,)), ((), ())), preferred_element_type=jnp.float32,
+        )
+
+    def x_copy(j):
+        return (remote(S.at[j], R.at[j], x_send.at[j], x_recv.at[j], to_x),)
+
+    def z_copy(j):
+        return (remote(ZS.at[j], ZR.at[j], z_send.at[j], z_recv.at[j], to_z),)
+
+    def pass_on(j):
+        arrive(x_copy(j))
+        ZS[j] = (PZ[j] + R[j, count:].astype(jnp.float32)).astype(jnp.bfloat16)
+        go(z_copy(j))
+        ACC[j] = ACC[j] + R[j, :count].astype(jnp.float32)
+
+    for j in range(DOWN_CUTS):
+        arrive(dn_copy(6, j))
+        go(dn_copy(7, j))
+        if j + 1 < DOWN_CUTS:
+            arrive(dn_copy(4, j + 1))
+            go(dn_copy(6, j + 1))
+            go(dn_copy(5, j + 1))
+        for k in (1, 3, 5, 7):
+            arrive(dn_copy(k, j))
+        S[j, count:] = down(3, j).astype(jnp.bfloat16)
+        S[j, :count] = down(2, j).astype(jnp.bfloat16)
+        go(x_copy(j))
+        PZ[j] = down(1, j)
+        ACC[j] = down(0, j)
+        if j:
+            pass_on(j - 1)
+    pass_on(DOWN_CUTS - 1)
+    square = jnp.zeros((count, 1), jnp.float32)
+    for j in range(DOWN_CUTS):
+        arrive(z_copy(j))
+        mixed = ACC[j] + ZR[j].astype(jnp.float32)
+        ACC[j] = mixed
+        square = square + jnp.sum(mixed * mixed, axis=1, keepdims=True)
+    scale = lax.rsqrt(square / width + 1e-06)
+    for j in range(DOWN_CUTS):
+        cols = pl.ds(j * d_rows, d_rows)
+        out[:, cols] = (ACC[j] * scale * post[:, cols]).astype(jnp.bfloat16)
+    for copy in sent:
+        copy.wait_send()
+
+
+def fused(n_ep, tokens, pre_gain, post_gain, expert_ids, route_weight, w_gate, w_up, w_down):
+    count, width = tokens.shape
+    part = w_gate.shape[2]
+    experts = n_ep * w_gate.shape[0]
+    names = jnp.arange(experts, dtype=jnp.int32)[:, None, None]
+    picks = jnp.where(expert_ids.T[None] == names, route_weight.T[None], 0.0)
+    wr = jnp.sum(picks, axis=1)
+    bf, f32 = jnp.bfloat16, jnp.float32
+    cols = width // DOWN_CUTS
+    anywhere = pl.BlockSpec(memory_space=pl.ANY)
+    vmem = pl.BlockSpec(memory_space=pltpu.VMEM)
+    dma = pltpu.SemaphoreType.DMA
+    return pl.pallas_call(
+        functools.partial(kernel, n_ep),
+        out_shape=jax.ShapeDtypeStruct((count, width), bf),
+        in_specs=[anywhere, vmem, vmem, anywhere, anywhere, anywhere, anywhere],
+        out_specs=vmem,
+        scratch_shapes=[
+            pltpu.VMEM((4, count, width), bf),
+            pltpu.VMEM((4, count, width), bf),
+            pltpu.VMEM((4, experts, count), f32),
+            pltpu.VMEM((2, 4 * count, part), f32),
+            pltpu.VMEM((8, width, 2 * part), bf),
+            pltpu.VMEM((width, 8 * part), bf),
+            pltpu.VMEM((4 * count, 8 * part), bf),
+            pltpu.VMEM((DOWN_CUTS, 2 * count, cols), bf),
+            pltpu.VMEM((DOWN_CUTS, 2 * count, cols), bf),
+            pltpu.VMEM((DOWN_CUTS, count, cols), f32),
+            pltpu.VMEM((DOWN_CUTS, count, cols), bf),
+            pltpu.VMEM((DOWN_CUTS, count, cols), bf),
+            pltpu.VMEM((DOWN_CUTS, count, cols), f32),
+            dma((5,)),
+            dma((4,)), dma((4,)), dma((4,)), dma((4,)),
+            dma((8, GU_CUTS)), dma((8, GU_CUTS)), dma((8, DOWN_CUTS)), dma((8, DOWN_CUTS)),
+            dma((DOWN_CUTS,)), dma((DOWN_CUTS,)), dma((DOWN_CUTS,)), dma((DOWN_CUTS,)),
+        ],
+        compiler_params=pltpu.CompilerParams(
+            collective_id=0, has_side_effects=True, vmem_limit_bytes=VMEM_BYTES
+        ),
+    )(tokens, pre_gain[None], post_gain[None], wr, w_gate, w_up, w_down)
+
+
+def whole_body(n_ep, n_tp, *args):
+    lanes = args[5].shape[2]
+    if n_ep // 2 == n_tp == 2 * 2 and args[5].shape[0] == 1 and lanes % 128 == 0:
+        return fused(n_ep, *args)
+    return body(*args)
+
 
 def solution(mesh):
     in_specs = (
@@ -63,4 +341,5 @@
         P("ep", None, "tp"),
     )
     out_specs = P(("ep", "tp"), None)
-    return jax.shard_map(body, mesh=mesh, in_specs=in_specs, out_specs=out_specs, check_vma=False)
+    step = functools.partial(whole_body, mesh.shape["ep"], mesh.shape["tp"])
+    return jax.shard_map(step, mesh=mesh, in_specs=in_specs, out_specs=out_specs, check_vma=False)

time: 264 us -> 147 us (0.56)
  waiting for transfers between devices: 186 us -> 0 us
  Pallas kernels: 0 us -> 143 us
  local copies, waits for them, and re-layouts: 21.9 us -> 3 us
  matrix products: 15.3 us -> 0 us
  other arithmetic: 14.1 us -> 0.6 us
  between operations: 13.3 us -> 0.01 us
  starting transfers between devices: 12.2 us -> 0 us
    all_to_all x2 -> x0, waiting for transfers between devices: 180 us -> none  [the longest x1 92.3 us: body(): lax.all_to_all(answer, 'ep', split_axis=0, concat_axis=0, tiled=True)]
    pallas_call x0 -> x1, Pallas kernels: none -> 143 us  [fused(): pl.pallas_call(functools.partial(kernel, n_ep), out_shape=jax.ShapeDtypeS...]
    dot_general x2 -> x0, matrix products: 15.3 us -> none  [the longest x1 10.1 us: expert_terms(): lax.dot_general(hidden, down_part, (((1,), (1,)), ((), ())), preferred_el...]
    gather x2 -> x0, local copies, waits for them, and re-layouts: 13.2 us -> none  [the longest x1 7.13 us: body(): returned.reshape(experts * capacity, width)[target]]
    all_to_all x2 -> x0, starting transfers between devices: 12.1 us -> none  [the longest x1 7.28 us: body(): lax.all_to_all(outgoing, 'ep', split_axis=0, concat_axis=0, tiled=True)]
    reduce_sum x4 -> x1, other arithmetic: 10.7 us -> 0.6 us  [fused(): wr = jnp.sum(picks, axis=1)]
    all_gather x3 -> x0, waiting for transfers between devices: 4.43 us -> none  [the longest x1 4.39 us: collect_expert(): lax.all_gather(w_up, 'tp', axis=2, tiled=True)]
    convert_element_type x1 -> x0, local copies, waits for them, and re-layouts: 4 us -> none  [body(): per_route.astype(jnp.float32) * route_weight[:, :, None]]
  transfers between devices with their start and end apart: 5 -> 0, of which waited for: 3 -> 0; matrix products, arithmetic and copies ran while one was open for 7% -> 0% of each run, Pallas kernels for 0% -> 0%
where the time goes in v1:
time: 147 us; the launch traced here: 146 us
  Pallas kernels  143 us (97%)
  local copies, waits for them, and re-layouts  3 us (2%)
    pallas_call x1, Pallas kernels, fused(): pl.pallas_call(functools.partial(kernel, n_ep), out_shape=jax.ShapeDtypeS...  143 us
    unnamed x5, local copies, waits for them, and re-layouts  3 us

profile of v1, /device:TPU:0, one launch (start us, length us, event | category | flops | bytes accessed | tf_op | source)
XLA Modules:
  0.0 146.4 jit_solution(1675900542922860104)
XLA Ops:
  0.0 0.0 copy-start.1
  0.0 0.0 copy-start
  0.0 0.7 copy-done.1
  0.7 0.0 copy-done
  0.7 0.6 select_reduce_fusion.wr
  1.3 142.8 %shard_map.82 = bf16[256,2048]{1,0:T(8,128)(2,1)} custom-call(bf16[256,2048]{1,0:T(8,128)(2,1)} %tok.1, f32[1,2048]{1,0:T(1,128)} %bitcast.4, f32[1,2048]{1,0:T(1,128)} %bitcast.5, f32[8,256]{1,0:T(8,128)} %select_reduce_fusion.wr, bf16[1,2048,128]{2,1,0:T(8,128)(2,1)} %wg.1, bf16[1,2048,128]{2,1,0:T(8,128)(2,1)} %wu.1, bf16[1,2048,128]{2,1,0:T(8,128)(2,1)} %wd.1), custom_call_target="tpu_custom_call" | custom-call | tf_op jit(solution)/shard_map/pallas_call | solution.py:295
  144.1 2.3 %copy.10 = bf16[256,2048]{1,0:T(8,128)(2,1)} copy(bf16[256,2048]{1,0:T(8,128)(2,1)} %shard_map.82) | data formatting | bytes 2097152
Async XLA Ops:
  0.0 0.7 copy-start.1
  0.0 0.7 copy-start

commit v2 on v1

--- a/solution.py
+++ b/solution.py
@@ -55,8 +55,10 @@
     return rms_scale(mixed, post_gain).astype(jnp.bfloat16)
 
 MESH = pl.DeviceIdType.MESH
-GU_CUTS = 2
-DOWN_CUTS = 4
+GU_CUTS = 8
+DOWN_CUTS = 8
+LAG = 5
+TOKEN_CUTS = 8
 VMEM_BYTES = 60 * 2**20
 
 
@@ -99,12 +101,16 @@
     block_from = {1: (0, to_z), 2: (0, to_x), 3: (1, to_x)}
     sent = []
 
-    def tokens_copy(k):
+    def routes_copy(k):
         s, who = block_from[k]
-        return (
-            remote(WR.at[s], WR.at[k], w_send.at[k], w_recv.at[k], who),
-            remote(T.at[s], T.at[k], t_send.at[k], t_recv.at[k], who),
-        )
+        return (remote(WR.at[s], WR.at[k], w_send.at[k], w_recv.at[k], who),)
+
+    t_rows = count // TOKEN_CUTS
+
+    def tokens_copy(k, j):
+        s, who = block_from[k]
+        rows = pl.ds(j * t_rows, t_rows)
+        return (remote(T.at[s, rows], T.at[k, rows], t_send.at[k, j], t_recv.at[k, j], who),)
 
     def route(k):
         if k % 2:
@@ -145,7 +151,7 @@
         def some(i, carry):
             part_rows = pl.ds(pl.multiple_of(i * 32, 32), 32)
             values = T[block, part_rows, :].astype(jnp.float32)
-            X[block, part_rows, :] = rms_scale(values, pre[...]).astype(jnp.bfloat16)
+            X[pl.ds(pl.multiple_of(block * count + i * 32, 32), 32), :] = rms_scale(values, pre[...]).astype(jnp.bfloat16)
             return carry
 
         lax.fori_loop(0, count // 32, some, 0)
@@ -163,70 +169,105 @@
     def hidden(slots, blocks):
         low, high = slots
         first, last = blocks
-        span = last - first
-
-        def one(i, carry):
-            s = low + lax.div(i, span)
-            b = first + lax.rem(i, span)
-            rows = pl.ds(pl.multiple_of(b * count, count), count)
-            both = jnp.dot(X[b], GU[s], preferred_element_type=jnp.float32)
+        rows = pl.ds(first * count, (last - first) * count)
+
+        def one(s, carry):
+            left = X[rows, :]
+            both = jnp.dot(left, GU[s], preferred_element_type=jnp.float32)
             gate, up = both[:, :part], both[:, part:]
             value = gate / (1.0 + jnp.exp(-gate)) * up * COL[lax.div(s, 4), rows, :]
             H[rows, pl.ds(pl.multiple_of(s * part, part), part)] = value.astype(jnp.bfloat16)
             return carry
 
-        lax.fori_loop(0, (high - low) * span, one, 0)
+        lax.fori_loop(low, high, one, 0)
 
     for copy in own[:2]:
         copy.wait()
     pl.semaphore_wait(barrier, 5)
-    go(tokens_copy(1))
-    go(tokens_copy(2))
+    for k in (1, 2):
+        go(routes_copy(k))
     for copy in own[2:4]:
         copy.wait()
-    for j in range(GU_CUTS):
-        for k in (4, 2, 1):
-            go(gu_copy(k, j))
+    for j in range(TOKEN_CUTS):
+        go(tokens_copy(1, j))
+        go(tokens_copy(2, j))
+        for i in range(j * GU_CUTS // TOKEN_CUTS, (j + 1) * GU_CUTS // TOKEN_CUTS):
+            for k in (4, 2, 1):
+                go(gu_copy(k, i))
     own[4].wait()
     for j in range(DOWN_CUTS):
-        for k in (4, 2, 1):
-            go(dn_copy(k, j))
+        go(dn_copy(1, j))
     norm(0)
     for j in range(GU_CUTS):
         arrive(gu_copy(1, j))
     hidden((0, 2), (0, 1))
-    arrive(tokens_copy(1))
-    go(tokens_copy(3))
-    norm(1)
+    arrive(routes_copy(1))
+    go(routes_copy(3))
+    arrive(routes_copy(2))
+
+    def tokens_on(low, high):
+        for i in range(low, high):
+            arrive(tokens_copy(1, i))
+            go(tokens_copy(3, i))
+
+    half_t, half_g = TOKEN_CUTS // 2, GU_CUTS // 2
+    tokens_on(0, half_t)
     for j in range(GU_CUTS):
         arrive(gu_copy(2, j))
         go(gu_copy(3, j))
-    arrive(tokens_copy(2))
+    for j in range(TOKEN_CUTS):
+        arrive(tokens_copy(2, j))
+
+    def fourth(low, high):
+        for j in range(low, high):
+            arrive(gu_copy(4, j))
+            go(gu_copy(6, j))
+            go(gu_copy(5, j))
+            span = TOKEN_CUTS - half_t
+            tokens_on(half_t + span * j // GU_CUTS, half_t + span * (j + 1) // GU_CUTS)
+
+    fourth(0, half_g)
     norm(2)
-    hidden((0, 2), (1, 3))
-    for j in range(GU_CUTS):
-        arrive(gu_copy(4, j))
-        go(gu_copy(6, j))
-        go(gu_copy(5, j))
+    fourth(half_g, half_g + 1)
+    hidden((0, 2), (2, 3))
     for j in range(GU_CUTS):
         arrive(gu_copy(3, j))
-    hidden((2, 4), (0, 3))
-    for j in range(DOWN_CUTS):
-        arrive(dn_copy(2, j))
-        go(dn_copy(3, j))
+    fourth(half_g + 1, half_g + 2)
+    hidden((2, 4), (0, 1))
+    fourth(half_g + 2, half_g + 3)
+    hidden((2, 4), (2, 3))
+    fourth(half_g + 3, GU_CUTS)
+    for j in range(DOWN_CUTS):
+        go(dn_copy(4, j))
+    go(dn_copy(2, 0))
+    go(dn_copy(2, 1))
+    norm(1)
     for j in range(GU_CUTS):
         arrive(gu_copy(5, j))
-    hidden((4, 6), (0, 3))
-    arrive(tokens_copy(3))
-    norm(3)
-    hidden((0, 6), (3, 4))
-    for j in range(GU_CUTS):
+    for j in range(GU_CUTS // 2):
         arrive(gu_copy(6, j))
         go(gu_copy(7, j))
-    arrive(dn_copy(4, 0))
-    go(dn_copy(6, 0))
-    go(dn_copy(5, 0))
-    hidden((6, 7), (0, 4))
+    hidden((0, 6), (1, 2))
+    for j in range(GU_CUTS // 2, GU_CUTS):
+        arrive(gu_copy(6, j))
+        go(gu_copy(7, j))
+    hidden((4, 6), (0, 1))
+    hidden((4, 6), (2, 3))
+    down_next = lambda j: (arrive(dn_copy(4, j)), go(dn_copy(6, j)), go(dn_copy(5, j)))
+    arrive(routes_copy(3))
+    for j in range(TOKEN_CUTS):
+        arrive(tokens_copy(3, j))
+    norm(3)
+    down_next(0)
+    go(dn_copy(2, 2))
+    hidden((0, 7), (3, 4))
+    hidden((6, 7), (0, 3))
+    arrive(dn_copy(2, 0))
+    go(dn_copy(3, 0))
+    down_next(1)
+    go(dn_copy(2, 3))
+    arrive(dn_copy(6, 0))
+    go(dn_copy(7, 0))
     for j in range(GU_CUTS):
         arrive(gu_copy(7, j))
     hidden((7, 8), (0, 4))
@@ -237,38 +278,43 @@
             (((1,), (1,)), ((), ())), preferred_element_type=jnp.float32,
         )
 
-    def x_copy(j):
-        return (remote(S.at[j], R.at[j], x_send.at[j], x_recv.at[j], to_x),)
-
-    def z_copy(j):
-        return (remote(ZS.at[j], ZR.at[j], z_send.at[j], z_recv.at[j], to_z),)
+    def first_copy(j):
+        return (remote(S.at[j], R.at[j], x_send.at[j], x_recv.at[j], to_z if j % 2 else to_x),)
+
+    def second_copy(j):
+        return (remote(ZS.at[j], ZR.at[j], z_send.at[j], z_recv.at[j], to_x if j % 2 else to_z),)
 
     def pass_on(j):
-        arrive(x_copy(j))
+        arrive(first_copy(j))
         ZS[j] = (PZ[j] + R[j, count:].astype(jnp.float32)).astype(jnp.bfloat16)
-        go(z_copy(j))
+        go(second_copy(j))
         ACC[j] = ACC[j] + R[j, :count].astype(jnp.float32)
 
     for j in range(DOWN_CUTS):
-        arrive(dn_copy(6, j))
-        go(dn_copy(7, j))
+        if j + 2 < DOWN_CUTS:
+            down_next(j + 2)
+        if j + 4 < DOWN_CUTS:
+            go(dn_copy(2, j + 4))
         if j + 1 < DOWN_CUTS:
-            arrive(dn_copy(4, j + 1))
-            go(dn_copy(6, j + 1))
-            go(dn_copy(5, j + 1))
+            arrive(dn_copy(2, j + 1))
+            go(dn_copy(3, j + 1))
+            arrive(dn_copy(6, j + 1))
+            go(dn_copy(7, j + 1))
         for k in (1, 3, 5, 7):
             arrive(dn_copy(k, j))
+        near, kept = (1, 2) if j % 2 else (2, 1)
         S[j, count:] = down(3, j).astype(jnp.bfloat16)
-        S[j, :count] = down(2, j).astype(jnp.bfloat16)
-        go(x_copy(j))
-        PZ[j] = down(1, j)
+        S[j, :count] = down(near, j).astype(jnp.bfloat16)
+        go(first_copy(j))
+        PZ[j] = down(kept, j)
         ACC[j] = down(0, j)
-        if j:
-            pass_on(j - 1)
-    pass_on(DOWN_CUTS - 1)
+        if j >= LAG:
+            pass_on(j - LAG)
+    for j in range(DOWN_CUTS - LAG, DOWN_CUTS):
+        pass_on(j)
     square = jnp.zeros((count, 1), jnp.float32)
     for j in range(DOWN_CUTS):
-        arrive(z_copy(j))
+        arrive(second_copy(j))
         mixed = ACC[j] + ZR[j].astype(jnp.float32)
         ACC[j] = mixed
         square = square + jnp.sum(mixed * mixed, axis=1, keepdims=True)
@@ -299,7 +345,7 @@
         out_specs=vmem,
         scratch_shapes=[
             pltpu.VMEM((4, count, width), bf),
-            pltpu.VMEM((4, count, width), bf),
+            pltpu.VMEM((4 * count, width), bf),
             pltpu.VMEM((4, experts, count), f32),
             pltpu.VMEM((2, 4 * count, part), f32),
             pltpu.VMEM((8, width, 2 * part), bf),
@@ -312,7 +358,7 @@
             pltpu.VMEM((DOWN_CUTS, count, cols), bf),
             pltpu.VMEM((DOWN_CUTS, count, cols), f32),
             dma((5,)),
-            dma((4,)), dma((4,)), dma((4,)), dma((4,)),
+            dma((4, TOKEN_CUTS)), dma((4, TOKEN_CUTS)), dma((4,)), dma((4,)),
             dma((8, GU_CUTS)), dma((8, GU_CUTS)), dma((8, DOWN_CUTS)), dma((8, DOWN_CUTS)),
             dma((DOWN_CUTS,)), dma((DOWN_CUTS,)), dma((DOWN_CUTS,)), dma((DOWN_CUTS,)),
         ],

time: 147 us -> 121 us (0.82)
  Pallas kernels: 143 us -> 116 us
    pallas_call x1, Pallas kernels: 143 us -> 116 us  [fused(): pl.pallas_call(functools.partial(kernel, n_ep), out_shape=jax.ShapeDtypeS...]
where the time goes in v2:
time: 121 us; the launch traced here: 119 us
  Pallas kernels  116 us (96%)
  local copies, waits for them, and re-layouts  3 us (2%)
    pallas_call x1, Pallas kernels, fused(): pl.pallas_call(functools.partial(kernel, n_ep), out_shape=jax.ShapeDtypeS...  116 us
    unnamed x5, local copies, waits for them, and re-layouts  3 us

profile of v2, /device:TPU:0, one launch (start us, length us, event | category | flops | bytes accessed | tf_op | source)
XLA Modules:
  0.0 119.4 jit_solution(5759111582034399667)
XLA Ops:
  0.0 0.0 copy-start.1
  0.0 0.0 copy-start
  0.0 0.7 copy-done.1
  0.7 0.0 copy-done
  0.7 0.6 select_reduce_fusion.wr
  1.3 115.8 %shard_map.82 = bf16[256,2048]{1,0:T(8,128)(2,1)} custom-call(bf16[256,2048]{1,0:T(8,128)(2,1)} %tok.1, f32[1,2048]{1,0:T(1,128)} %bitcast.4, f32[1,2048]{1,0:T(1,128)} %bitcast.5, f32[8,256]{1,0:T(8,128)} %select_reduce_fusion.wr, bf16[1,2048,128]{2,1,0:T(8,128)(2,1)} %wg.1, bf16[1,2048,128]{2,1,0:T(8,128)(2,1)} %wu.1, bf16[1,2048,128]{2,1,0:T(8,128)(2,1)} %wd.1), custom_call_target="tpu_custom_call" | custom-call | tf_op jit(solution)/shard_map/pallas_call | solution.py:341
  117.1 2.3 %copy.10 = bf16[256,2048]{1,0:T(8,128)(2,1)} copy(bf16[256,2048]{1,0:T(8,128)(2,1)} %shard_map.82) | data formatting | bytes 2097152
Async XLA Ops:
  0.0 0.7 copy-start.1
  0.0 0.7 copy-start
